TPU v7x, 512 devices: a whole 4x8x8 slice. The times are simulated.
512 devices in a mesh: sp: 32 (over z, x), tp: 16 (over y, core).
Axes of the slice: x: 4, y: 8, z: 8, core: 2. Of those that a mesh axis runs over, the one named last changes fastest.
Arguments:
- moe_input: bfloat16 [6144, 2048], P('sp'), may hold values from -6 to 6
- out_grad: bfloat16 [6144, 2048], P('sp', 'tp'), may hold values from -6 to 6
- expert_ids: int32 [6144, 2], P('sp'), may hold values from 0 to 31, all different within a row; in each aligned block of 192 rows (0 to 191, 192 to 383, ...) at most 15 rows name the same one
- expert_weights: float32 [6144, 2], P('sp'), may hold values from 0.1 to 0.9
- w_gate: bfloat16 [32, 2048, 2048], P('sp', None, 'tp'), may hold values from -0.125 to 0.125
- w_up: bfloat16 [32, 2048, 2048], P('sp', None, 'tp'), may hold values from -0.125 to 0.125
- w_down: bfloat16 [32, 2048, 2048], P('sp', 'tp'), may hold values from -0.125 to 0.125
- out_proj: bfloat16 [1536, 2048], P('tp'), may hold values from -0.15625 to 0.15625
- retained: bfloat16 [6144, 1536], P('sp', 'tp'), may hold values from -6 to 6
- queries: bfloat16 [6144, 768], P('sp', 'tp'), may hold values from -6 to 6
- keys: bfloat16 [6144, 768], P('sp', 'tp'), may hold values from -0.86328125 to 0.86328125
- values: bfloat16 [6144, 1536], P('sp', 'tp'), may hold values from -6 to 6
- log_decay: float32 [6144, 16], P('sp', 'tp'), may hold values from -1 to 0
- incoming_state: float32 [32, 16, 48, 96], P('sp', 'tp'), may hold values from -6 to 6
Outputs:
- w_gate_grad: bfloat16 [32, 2048, 2048], P('sp', None, 'tp')
- w_up_grad: bfloat16 [32, 2048, 2048], P('sp', None, 'tp')
- w_down_grad: bfloat16 [32, 2048, 2048], P('sp', 'tp')
- out_proj_grad: float32 [2048, 1536], P('sp', 'tp')
- query_grad: bfloat16 [6144, 768], P('sp', 'tp')
- key_grad: bfloat16 [6144, 768], P('sp', 'tp')
- value_grad: bfloat16 [6144, 1536], P('sp', 'tp')
Inputs may be any that keep to these rules, and one draw needn't show every extreme that they name: `expert_ids`: in each aligned block of 192 positions no expert is named by more than 15 of the block's assignments, a bound that some block reaches.
All inputs are finite; a program needn't handle non-finite values.
Results may differ from a plain program's by a relative error of at most 0.02.
Values may be sent and summed in bfloat16 or wider, within the bound.
No kernel may reach another device: no remote copies, remote signals or barrier semaphores. Data moves between devices by JAX's collectives and lax.ppermute only.
A program may use at most 64 MiB of HBM per device.

v0:
```python
import jax
import jax.numpy as jnp
from jax import lax
from jax.sharding import Mesh
from jax.sharding import PartitionSpec as P

TP = ("y", "c")
F32 = jnp.float32
BF16 = jnp.bfloat16
ACROSS = (((1,), (1,)), ((), ()))
ALONG = (((0,), (0,)), ((), ()))
SWAP = [(0, 1), (1, 0)]


def dot(a, b, dims=(((1,), (0,)), ((), ()))):
    return lax.dot_general(a, b, dims, preferred_element_type=F32)


def slot_tables(expert_ids, expert_weights, experts, capacity, padded):
    tokens = expert_ids.shape[0]
    ids = expert_ids.T
    weights = expert_weights.T
    names = jnp.arange(experts, dtype=jnp.int32)[:, None]
    onehot = [(names == ids[j][None, :]).astype(BF16) for j in (0, 1)]
    place = jnp.arange(tokens)
    earlier = (place[:, None] < place[None, :]).astype(BF16)
    before = dot(onehot[0] + onehot[1], earlier)
    slots = jnp.arange(experts * padded, dtype=jnp.int32)[:, None]
    picker, slot_weight = (0.0, 0.0)
    for j in (0, 1):
        rank = jnp.sum(before * onehot[j].astype(F32), axis=0).astype(jnp.int32)
        hits = slots == (ids[j] * padded + rank)[None, :]
        picker = picker + jnp.where(hits, 1.0, 0.0)
        slot_weight = slot_weight + jnp.sum(
            jnp.where(hits, weights[j][None, :], 0.0), axis=1, keepdims=True
        )
    return (picker.astype(BF16), slot_weight)


def parity_columns(x, index):
    rows, cols = x.shape
    return lax.dynamic_index_in_dim(
        x.reshape(rows, 8, 2, cols // 16), index, 2, keepdims=False
    ).reshape(rows, cols // 2)


def parity_rows(x, index):
    rows, cols = x.shape
    return lax.dynamic_index_in_dim(
        x.reshape(8, 2, rows // 16, cols), index, 1, keepdims=False
    ).reshape(rows // 2, cols)


def joined_rows(own, other, core):
    rows, cols = own.shape
    own, other = (a.reshape(8, 1, rows // 8, cols) for a in (own, other))
    first = jnp.where(core == 0, own, other)
    second = jnp.where(core == 0, other, own)
    return jnp.concatenate([first, second], axis=1).reshape(2 * rows, cols)


def joined_columns(own, other, core):
    rows, cols = own.shape
    own, other = (a.reshape(rows, 8, 1, cols // 8) for a in (own, other))
    first = jnp.where(core == 0, own, other)
    second = jnp.where(core == 0, other, own)
    return jnp.concatenate([first, second], axis=2).reshape(rows, 2 * cols)


def in_three(x):
    high = x.astype(BF16)
    rest = x - high.astype(F32)
    middle = rest.astype(BF16)
    low = (rest - middle.astype(F32)).astype(BF16)
    return (high, middle, low)


def on_device(
    moe_input,
    out_grad,
    expert_ids,
    expert_weights,
    w_gate,
    w_up,
    w_down,
    out_proj,
    retained,
    queries,
    keys,
    values,
    log_decay,
    incoming_state,
):
    tokens = moe_input.shape[0]
    width = moe_input.shape[1]
    sp_count = lax.axis_size("sp")
    capacity = 5 * tokens // (2 * sp_count)
    padded = 16
    slot_count = sp_count * capacity
    core = lax.axis_index("c")
    block = lax.axis_index("sp")
    chunk = out_grad.shape[1]
    running = jnp.cumsum(log_decay[:, 0])
    last = running[-1]
    picker, slot_weight = slot_tables(expert_ids, expert_weights, sp_count, capacity, padded)
    mine = parity_columns(moe_input, core)
    send_rows = dot(picker, mine).astype(BF16).reshape(sp_count, padded, -1)
    parts = in_three(last)
    lane = jnp.arange(chunk)[None, None, :]
    extra = jnp.where(
        lane == 0, parts[0], jnp.where(lane == 1, parts[1], jnp.where(lane == 2, parts[2], 0.0))
    ).astype(BF16)
    send_grad = (dot(picker, out_grad) * slot_weight).astype(BF16).reshape(sp_count, padded, -1)
    spot = jnp.arange(padded)[None, :, None]
    send_grad = jnp.where(spot == padded - 1, extra, send_grad)
    got_grad = lax.all_to_all(send_grad, "sp", 0, 0, tiled=True)
    got_rows = lax.all_to_all(send_rows, "sp", 0, 0, tiled=True)
    rows_own = got_rows[:, :capacity].reshape(slot_count, -1)
    grad_part = got_grad[:, :capacity].reshape(slot_count, -1)
    ends = jnp.sum(got_grad[:, capacity, :3].astype(F32), axis=1)
    grad_own = lax.all_gather(grad_part, "y", axis=1, tiled=True)
    rows_other = lax.ppermute(rows_own, "c", SWAP)
    grad_other = lax.ppermute(grad_own, "c", SWAP)
    gate_own, gate_other = (parity_rows(w_gate[0], k) for k in (core, 1 - core))
    up_own, up_other = (parity_rows(w_up[0], k) for k in (core, 1 - core))
    down_own, down_other = (parity_columns(w_down[0], k) for k in (core, 1 - core))
    gate = dot(rows_own, gate_own) + dot(rows_other, gate_other)
    up = dot(rows_own, up_own) + dot(rows_other, up_other)
    sig = jax.nn.sigmoid(gate)
    swish = gate * sig
    act = (swish * up).astype(BF16)
    act_grad = dot(grad_own, down_own, ACROSS) + dot(grad_other, down_other, ACROSS)
    gate_grad = (act_grad * up * sig * (1.0 + gate * (1.0 - sig))).astype(BF16)
    up_grad = (act_grad * swish).astype(BF16)
    partial_other = (dot(gate_grad, gate_other, ACROSS) + dot(up_grad, up_other, ACROSS)).astype(
        BF16
    )
    arrived = lax.ppermute(partial_other, "c", SWAP)
    partial_own = dot(gate_grad, gate_own, ACROSS) + dot(up_grad, up_own, ACROSS)
    pair = (partial_own + arrived.astype(F32)).astype(BF16)
    pieces = jnp.moveaxis(pair.reshape(slot_count, 8, chunk), 1, 0)
    pieces = lax.all_to_all(pieces, "y", 0, 0, tiled=True)
    share = jnp.sum(pieces.astype(F32), axis=0).astype(BF16)
    gate_w_grad = joined_rows(
        dot(rows_own, gate_grad, ALONG).astype(BF16),
        dot(rows_other, gate_grad, ALONG).astype(BF16),
        core,
    )
    up_w_grad = joined_rows(
        dot(rows_own, up_grad, ALONG).astype(BF16),
        dot(rows_other, up_grad, ALONG).astype(BF16),
        core,
    )
    down_grad = joined_columns(
        dot(act, grad_own, ALONG).astype(BF16), dot(act, grad_other, ALONG).astype(BF16), core
    )
    returned = lax.all_to_all(share.reshape(sp_count, capacity, chunk), "sp", 0, 0, tiled=True)
    returned = jnp.pad(returned, ((0, 0), (0, padded - capacity), (0, 0)))
    token_grad = dot(picker, returned.reshape(sp_count * padded, chunk), ALONG)
    stream_part = (out_grad.astype(F32) + token_grad).astype(BF16)
    stream = lax.all_gather(stream_part, TP, axis=1, tiled=True)
    ret_grad = dot(stream, out_proj, ACROSS).astype(BF16)
    q, k, v, o = (a.astype(F32) for a in (queries, keys, values, ret_grad))
    rising = jnp.exp(running)[:, None]
    inject = dot(q * rising, o, ALONG)
    value_dim = values.shape[1]
    sent = jnp.broadcast_to(inject.astype(BF16)[None], (sp_count, *inject.shape))
    states = lax.all_to_all(sent, "sp", 0, 0, tiled=True)
    proj_part = dot(stream, retained, ALONG).astype(BF16)
    proj_parts = lax.all_to_all(
        proj_part.reshape(sp_count, width // sp_count, value_dim), "sp", 0, 0, tiled=True
    )
    out_proj_grad = jnp.sum(proj_parts.astype(F32), axis=0)
    order = jnp.arange(sp_count)
    between = (order[None, :] > block) & (order[None, :] < order[:, None])
    factors = jnp.where(
        order > block, jnp.exp(jnp.sum(jnp.where(between, ends[None, :], 0.0), axis=1)), 0.0
    )
    state_grad = jnp.sum(factors[:, None, None] * states.astype(F32), axis=0)
    place = jnp.arange(tokens)
    causal = place[:, None] >= place[None, :]
    diff = running[:, None] - running[None, :]
    decay = jnp.where(causal, jnp.exp(jnp.minimum(diff, 0.0)), 0.0)
    scores = dot(q, k, ACROSS) * decay
    prob_grad = dot(o, v, ACROSS) * decay
    tail = jnp.exp(last - running)[:, None]
    query_grad = dot(prob_grad, k) + rising * dot(o, incoming_state[0, 0], ACROSS)
    key_grad = dot(prob_grad, q, ALONG) + tail * dot(v, state_grad, ACROSS)
    value_grad = dot(scores, o, ALONG) + tail * dot(k, state_grad)
    return (
        gate_w_grad[None],
        up_w_grad[None],
        down_grad[None],
        out_proj_grad,
        query_grad.astype(BF16),
        key_grad.astype(BF16),
        value_grad.astype(BF16),
    )


def solution(mesh):
    torus = Mesh(mesh.devices.reshape(mesh.shape["sp"], 8, 2), ("sp", "y", "c"))
    placed = (
        P("sp", None),
        P("sp", TP),
        P("sp", None),
        P("sp", None),
        P("sp", None, TP),
        P("sp", None, TP),
        P("sp", TP, None),
        P(TP, None),
        P("sp", TP),
        P("sp", TP),
        P("sp", TP),
        P("sp", TP),
        P("sp", TP),
        P("sp", TP, None, None),
    )
    return jax.shard_map(
        on_device,
        mesh=torus,
        in_specs=placed,
        out_specs=(
            P("sp", None, TP),
            P("sp", None, TP),
            P("sp", TP, None),
            P("sp", TP),
            P("sp", TP),
            P("sp", TP),
            P("sp", TP),
        ),
        check_vma=False,
    )
```

profile of v0, /device:TPU:2, one launch (start us, length us, event | category | flops | bytes accessed | tf_op | source)
XLA Modules:
  0.0 204.9 jit_solution(3928460115457227741)
XLA Ops:
  0.7 0.8 pad_bitcast_fusion
  1.4 0.3 reduce-window.9
  2.1 0.6 slice.42
  4.0 0.8 fusion.40
  4.9 0.8 fusion.39
  5.7 0.8 multiply_add_fusion.1
  6.6 1.2 fusion.1
  7.8 0.7 broadcast_select_fusion.4
  8.6 13.5 %all-to-all-start.1 = ((bf16[32,16,128]{2,1,0:T(8,128)(2,1)}), bf16[32,16,128]{2,1,0:T(8,128)(2,1)S(1)}, u32[]{:S(2)}, u32[]{:S(2)}) async-start(bf16[32,16,128]{2,1,0:T(8,128)(2,1)} %broadcast_select_fusion.4), calls=%async_computation.1 | async-start | bytes 262144 | tf_op jit(solution)/shard_map/all_to_all | solution.py:116
  22.0 0.6 reshape.287
  22.6 2.3 %dynamic-slice_reduce_fusion = bf16[192,8,128]{2,1,0:T(8,128)(2,1)S(1)} fusion(bf16[192,8,2,128]{3,2,1,0:T(2,128)(2,1)S(1)} %reshape.287, s32[]{:T(128)S(6)} %select_n.175), kind=kLoop, calls=%fused_computation.37 | loop fusion | bytes 786436 | tf_op jit(solution)/shard_map/jit(dynamic_index_in_dim)/dynamic_slice | solution.py:42
  25.0 1.6 convolution_convert_fusion.1
  26.6 4.3 %all-to-all-done.1 = bf16[32,16,128]{2,1,0:T(8,128)(2,1)S(1)} async-done(((bf16[32,16,128]{2,1,0:T(8,128)(2,1)}), bf16[32,16,128]{2,1,0:T(8,128)(2,1)S(1)}, u32[]{:S(2)}, u32[]{:S(2)}) %all-to-all-start.1) | async-done | bytes 131104 | tf_op jit(solution)/shard_map/all_to_all | solution.py:116
  30.9 5.5 %all-to-all-start = ((bf16[32,16,1024]{2,1,0:T(8,128)(2,1)}), bf16[32,16,1024]{2,1,0:T(8,128)(2,1)S(1)}, u32[]{:S(2)}, u32[]{:S(2)}) async-start(bf16[32,16,1024]{2,1,0:T(8,128)(2,1)} %bitcast.7), calls=%async_computation | async-start | bytes 2097152 | tf_op jit(solution)/shard_map/all_to_all | solution.py:117
  36.4 28.7 %all_gather.6 = bf16[480,1024]{1,0:T(8,128)(2,1)S(1)} all-gather(bf16[480,128]{1,0:T(8,128)(2,1)S(1)} %reshape.294), channel_id=1, replica_groups=mesh['sp'=32,'y'=8,'c'=2] {'y'}, dimensions={1}, use_global_device_ids=true | all-gather | bytes 1105920 | tf_op jit(solution)/shard_map/all_gather | solution.py:121
  65.1 1.9 collective-permute-start
  67.0 1.3 copy.47
  68.3 0.8 constant_dynamic-slice_fusion.4
  69.2 2.2 %constant_dynamic-slice_fusion = (bf16[8,1,128,128]{3,2,1,0:T(8,128)(2,1)}, bf16[8,1,128,128]{3,2,1,0:T(8,128)(2,1)}, bf16[8,1,128,128]{3,2,1,0:T(8,128)(2,1)}, bf16[8,1,128,128]{3,2,1,0:T(8,128)(2,1)}) fusion(bf16[8,2,128,128]{3,2,1,0:T(8,128)(2,1)} %bitcast.158, s32[]{:T(128)S(6)} %select_n.182, s32[]{:T(128)S(6)} %select_n.175, ...), kind=kLoop, calls=%fused_computation.88 | loop fusion | bytes 2097160 | tf_op jit(solution)/shard_map/jit(dynamic_index_in_dim)/dynamic_slice | solution.py:49
  71.3 0.3 reshape.290
  71.7 2.5 %collective-permute-start.1 = (bf16[480,1024]{1,0:T(8,128)(2,1)S(1)}, bf16[480,1024]{1,0:T(8,128)(2,1)S(1)}, u32[]{:S(2)}, u32[]{:S(2)}) collective-permute-start(bf16[480,1024]{1,0:T(8,128)(2,1)S(1)} %reshape.290), channel_id=1, source_target_pairs={{0,1},{1,0},{2,3},{3,2},{4,5},{5,4},{6,7},{7,6},{8,9},{9,8},{10,11... | collective-permute-start | bytes 2949128 | tf_op jit(solution)/shard_map/ppermute | solution.py:122
  74.2 1.4 fusion.43
  75.6 1.7 convolution_add_fusion.2
  77.3 0.4 fusion.45
  77.8 0.4 fusion.44
  78.2 0.4 convolution_add_fusion
  78.7 1.1 multiply_convert_fusion
  79.8 0.4 fusion.47
  80.2 1.4 add_convert_fusion.1
  81.6 1.9 collective-permute-start.2
  83.6 0.7 subtract_exponential_fusion
  84.3 1.2 fusion.27
  85.6 1.4 fusion.46
  87.0 1.6 fusion
  88.6 1.1 copy.65
  89.7 4.4 %all-to-all-start.2 = ((bf16[8,480,128]{2,1,0:T(8,128)(2,1)}), bf16[8,480,128]{2,1,0:T(8,128)(2,1)}, u32[]{:S(2)}, u32[]{:S(2)}) async-start(bf16[8,480,128]{2,1,0:T(8,128)(2,1)} %bitcast.137), calls=%async_computation.2 | async-start | bytes 1966080 | tf_op jit(solution)/shard_map/all_to_all | solution.py:142
  94.2 1.2 convolution_convert_fusion.3
  95.4 1.6 select_bitcast_fusion.1
  97.2 1.6 copy.50
  98.8 2.2 %broadcast_in_dim_reshape.11 = bf16[1,128,2048]{2,1,0:T(8,128)(2,1)} reshape(bf16[128,8,2,128]{3,2,1,0:T(2,128)(2,1)} %copy.50) | data formatting | bytes 1048576 | tf_op jit(solution)/shard_map/broadcast_in_dim;reshape | solution.py:193
  101.0 0.5 convolution_convert_fusion.7
  101.5 0.5 convolution_convert_fusion.5
  102.0 0.5 broadcast_select_fusion.1
  102.5 0.5 broadcast_select_fusion.3
  103.0 16.8 %all-to-all-done.2 = bf16[8,480,128]{2,1,0:T(8,128)(2,1)} async-done(((bf16[8,480,128]{2,1,0:T(8,128)(2,1)}), bf16[8,480,128]{2,1,0:T(8,128)(2,1)}, u32[]{:S(2)}, u32[]{:S(2)}) %all-to-all-start.2) | async-done | bytes 983072 | tf_op jit(solution)/shard_map/all_to_all | solution.py:142
  119.9 1.3 reduce_sum.88
  121.2 0.7 reshape.302
  121.9 9.7 %all-to-all-start.3 = ((bf16[32,15,128]{2,1,0:T(8,128)(2,1)}), bf16[32,15,128]{2,1,0:T(8,128)(2,1)S(1)}, u32[]{:S(2)}, u32[]{:S(2)}) async-start(bf16[32,15,128]{2,1,0:T(8,128)(2,1)} %reshape.302), calls=%async_computation.3 | async-start | bytes 262144 | tf_op jit(solution)/shard_map/all_to_all | solution.py:157
  131.7 0.8 copy.48
  132.6 0.8 copy.49
  133.4 7.2 %all-to-all-done.3 = bf16[32,15,128]{2,1,0:T(8,128)(2,1)S(1)} async-done(((bf16[32,15,128]{2,1,0:T(8,128)(2,1)}), bf16[32,15,128]{2,1,0:T(8,128)(2,1)S(1)}, u32[]{:S(2)}, u32[]{:S(2)}) %all-to-all-start.3) | async-done | bytes 122912 | tf_op jit(solution)/shard_map/all_to_all | solution.py:157
  141.0 19.1 %all_gather.7 = bf16[192,2048]{1,0:T(8,128)(2,1)S(1)} all-gather(bf16[192,128]{1,0:T(8,128)(2,1)S(1)} %fusion.6), channel_id=1, replica_groups=mesh['sp'=32,'y'=8,'c'=2] {'y','c'}, dimensions={1}, use_global_device_ids=true | all-gather | bytes 835584 | tf_op jit(solution)/shard_map/all_gather | solution.py:161
  160.1 0.4 convolution_convert_fusion.8
  160.9 0.8 broadcast_in_dim.121
  161.7 5.6 %all-to-all-start.5 = ((bf16[32,48,96]{2,1,0:T(8,128)(2,1)}), bf16[32,48,96]{2,1,0:T(8,128)(2,1)S(1)}, u32[]{:S(2)}, u32[]{:S(2)}) async-start(bf16[32,48,96]{2,1,0:T(8,128)(2,1)} %broadcast_in_dim.121), calls=%async_computation.5 | async-start | bytes 786432 | tf_op jit(solution)/shard_map/all_to_all | solution.py:168
  167.7 1.0 copy.52
  168.8 0.5 fusion.2
  169.3 12.9 %all-to-all-done.5 = bf16[32,48,96]{2,1,0:T(8,128)(2,1)S(1)} async-done(((bf16[32,48,96]{2,1,0:T(8,128)(2,1)}), bf16[32,48,96]{2,1,0:T(8,128)(2,1)S(1)}, u32[]{:S(2)}, u32[]{:S(2)}) %all-to-all-start.5) | async-done | bytes 294944 | tf_op jit(solution)/shard_map/all_to_all | solution.py:168
  182.2 5.6 %all-to-all-start.4 = ((bf16[32,64,96]{2,1,0:T(8,128)(2,1)}), bf16[32,64,96]{2,1,0:T(8,128)(2,1)S(1)}, u32[]{:S(2)}, u32[]{:S(2)}) async-start(bf16[32,64,96]{2,1,0:T(8,128)(2,1)} %bitcast.33), calls=%async_computation.4 | async-start | bytes 1048576 | tf_op jit(solution)/shard_map/all_to_all | solution.py:170
  187.8 0.8 fusion.10
  188.8 0.8 fusion.11
  189.6 0.8 fusion.5
  190.4 13.7 %all-to-all-done.4 = bf16[32,64,96]{2,1,0:T(8,128)(2,1)S(1)} async-done(((bf16[32,64,96]{2,1,0:T(8,128)(2,1)}), bf16[32,64,96]{2,1,0:T(8,128)(2,1)S(1)}, u32[]{:S(2)}, u32[]{:S(2)}) %all-to-all-start.4) | async-done | bytes 393248 | tf_op jit(solution)/shard_map/all_to_all | solution.py:170
  204.1 0.7 convert_reduce_fusion
  (66 shorter events, 2.6 us)
Async XLA Ops:
  0.6 159.4 %copy-start = (bf16[96,2048]{1,0:T(8,128)(2,1)S(1)}, bf16[96,2048]{1,0:T(8,128)(2,1)}, u32[]{:S(2)}) copy-start(bf16[96,2048]{1,0:T(8,128)(2,1)} %param.21) | copy-start | bytes 1179652
  0.6 21.4 %copy-start.9 = (bf16[192,2048]{1,0:T(8,128)(2,1)S(1)}, bf16[192,2048]{1,0:T(8,128)(2,1)}, u32[]{:S(2)}) copy-start(bf16[192,2048]{1,0:T(8,128)(2,1)} %param.14) | copy-start | bytes 2359300
  8.6 22.3 %all-to-all-start.1 = ((bf16[32,16,128]{2,1,0:T(8,128)(2,1)}), bf16[32,16,128]{2,1,0:T(8,128)(2,1)S(1)}, u32[]{:S(2)}, u32[]{:S(2)}) async-start(bf16[32,16,128]{2,1,0:T(8,128)(2,1)} %broadcast_select_fusion.4), calls=%async_computation.1 | async-start | bytes 262144 | tf_op jit(solution)/shard_map/all_to_all | solution.py:116
  30.9 5.5 %copy-start.10 = (bf16[32,16,128]{2,1,0:T(8,128)(2,1)}, bf16[32,16,128]{2,1,0:T(8,128)(2,1)S(1)}, u32[]{:S(2)}) copy-start(bf16[32,16,128]{2,1,0:T(8,128)(2,1)S(1)} %all-to-all-done.1) | copy-start | bytes 393220
  30.9 40.4 %all-to-all-start = ((bf16[32,16,1024]{2,1,0:T(8,128)(2,1)}), bf16[32,16,1024]{2,1,0:T(8,128)(2,1)S(1)}, u32[]{:S(2)}, u32[]{:S(2)}) async-start(bf16[32,16,1024]{2,1,0:T(8,128)(2,1)} %bitcast.7), calls=%async_computation | async-start | bytes 2097152 | tf_op jit(solution)/shard_map/all_to_all | solution.py:117
  65.1 10.5 %collective-permute-start = (bf16[480,1024]{1,0:T(8,128)(2,1)S(1)}, bf16[480,1024]{1,0:T(8,128)(2,1)}, u32[]{:S(2)}, u32[]{:S(2)}) collective-permute-start(bf16[480,1024]{1,0:T(8,128)(2,1)S(1)} %all_gather.6), channel_id=1, source_target_pairs={{0,1},{1,0},{2,3},{3,2},{4,5},{5,4},{6,7},{7,6},{8,9},{9,8},{10,11... | collective-permute-start | bytes 2949128 | tf_op jit(solution)/shard_map/ppermute | solution.py:123
  71.6 5.7 %copy-start.3 = (bf16[8,1,128,128]{3,2,1,0:T(8,128)(2,1)S(1)}, bf16[8,1,128,128]{3,2,1,0:T(8,128)(2,1)}, u32[]{:S(2)}) copy-start(bf16[8,1,128,128]{3,2,1,0:T(8,128)(2,1)} %get-tuple-element.20) | copy-start | bytes 786436
  71.7 6.6 %collective-permute-start.1 = (bf16[480,1024]{1,0:T(8,128)(2,1)S(1)}, bf16[480,1024]{1,0:T(8,128)(2,1)S(1)}, u32[]{:S(2)}, u32[]{:S(2)}) collective-permute-start(bf16[480,1024]{1,0:T(8,128)(2,1)S(1)} %reshape.290), channel_id=1, source_target_pairs={{0,1},{1,0},{2,3},{3,2},{4,5},{5,4},{6,7},{7,6},{8,9},{9,8},{10,11... | collective-permute-start | bytes 2949128 | tf_op jit(solution)/shard_map/ppermute | solution.py:122
  75.6 2.2 %copy-start.1 = (bf16[8,1,128,128]{3,2,1,0:T(8,128)(2,1)S(1)}, bf16[8,1,128,128]{3,2,1,0:T(8,128)(2,1)}, u32[]{:S(2)}) copy-start(bf16[8,1,128,128]{3,2,1,0:T(8,128)(2,1)} %get-tuple-element.33) | copy-start | bytes 786436
  75.6 2.6 %copy-start.4 = (bf16[8,1,128,128]{3,2,1,0:T(8,128)(2,1)S(1)}, bf16[8,1,128,128]{3,2,1,0:T(8,128)(2,1)}, u32[]{:S(2)}) copy-start(bf16[8,1,128,128]{3,2,1,0:T(8,128)(2,1)} %get-tuple-element.19) | copy-start | bytes 786436
  77.8 1.0 copy-start.8
  79.8 1.8 copy-start.5
  81.6 5.3 %collective-permute-start.2 = (bf16[480,1024]{1,0:T(8,128)(2,1)}, bf16[480,1024]{1,0:T(8,128)(2,1)}, u32[]{:S(2)}, u32[]{:S(2)}) collective-permute-start(bf16[480,1024]{1,0:T(8,128)(2,1)} %add_convert_fusion.1), channel_id=1, source_target_pairs={{0,1},{1,0},{2,3},{3,2},{4,5},{5,4},{6,7},{7,6},{8,9},{9,8},{10,11... | collective-permute-start | bytes 2949128 | tf_op jit(solution)/shard_map/ppermute | solution.py:138
  83.6 3.4 %copy-start.2 = (bf16[8,1,128,128]{3,2,1,0:T(8,128)(2,1)S(1)}, bf16[8,1,128,128]{3,2,1,0:T(8,128)(2,1)}, u32[]{:S(2)}) copy-start(bf16[8,1,128,128]{3,2,1,0:T(8,128)(2,1)} %get-tuple-element.33) | copy-start | bytes 786436
  83.6 3.4 %copy-start.6 = (bf16[480,128]{1,0:T(8,128)(2,1)S(1)}, bf16[480,128]{1,0:T(8,128)(2,1)}, u32[]{:S(2)}) copy-start(bf16[480,128]{1,0:T(8,128)(2,1)} %copy-done.5) | copy-start | bytes 368644
  89.7 30.1 %all-to-all-start.2 = ((bf16[8,480,128]{2,1,0:T(8,128)(2,1)}), bf16[8,480,128]{2,1,0:T(8,128)(2,1)}, u32[]{:S(2)}, u32[]{:S(2)}) async-start(bf16[8,480,128]{2,1,0:T(8,128)(2,1)} %bitcast.137), calls=%async_computation.2 | async-start | bytes 1966080 | tf_op jit(solution)/shard_map/all_to_all | solution.py:142
  97.2 4.3 %copy-start.7 = (bf16[480,128]{1,0:T(8,128)(2,1)S(1)}, bf16[480,128]{1,0:T(8,128)(2,1)}, u32[]{:S(2)}) copy-start(bf16[480,128]{1,0:T(8,128)(2,1)} %copy-done.5) | copy-start | bytes 368644
  121.9 18.7 %all-to-all-start.3 = ((bf16[32,15,128]{2,1,0:T(8,128)(2,1)}), bf16[32,15,128]{2,1,0:T(8,128)(2,1)S(1)}, u32[]{:S(2)}, u32[]{:S(2)}) async-start(bf16[32,15,128]{2,1,0:T(8,128)(2,1)} %reshape.302), calls=%async_computation.3 | async-start | bytes 262144 | tf_op jit(solution)/shard_map/all_to_all | solution.py:157
  131.7 9.0 %copy-start.16 = (bf16[192,128]{1,0:T(8,128)(2,1)S(1)}, bf16[192,128]{1,0:T(8,128)(2,1)}, u32[]{:S(2)}) copy-start(bf16[192,128]{1,0:T(8,128)(2,1)} %param.15) | copy-start | bytes 147460
  132.6 27.9 %copy-start.13 = (bf16[192,96]{1,0:T(8,128)(2,1)S(1)}, bf16[192,96]{1,0:T(8,128)(2,1)}, u32[]{:S(2)}) copy-start(bf16[192,96]{1,0:T(8,128)(2,1)} %param.22) | copy-start | bytes 110596
  140.7 20.1 %copy-start.11 = (bf16[192,48]{0,1:T(8,128)(2,1)S(1)}, bf16[192,48]{0,1:T(8,128)(2,1)}, u32[]{:S(2)}) copy-start(bf16[192,48]{0,1:T(8,128)(2,1)} %param.23) | copy-start | bytes 55300
  160.1 7.3 %copy-start.14 = (bf16[192,96]{1,0:T(8,128)(2,1)S(1)}, bf16[192,96]{1,0:T(8,128)(2,1)}, u32[]{:S(2)}) copy-start(bf16[192,96]{1,0:T(8,128)(2,1)} %param.25) | copy-start | bytes 110596
  160.5 8.2 %copy-start.12 = (bf16[192,48]{0,1:T(8,128)(2,1)S(1)}, bf16[192,48]{0,1:T(8,128)(2,1)}, u32[]{:S(2)}) copy-start(bf16[192,48]{0,1:T(8,128)(2,1)} %param.24) | copy-start | bytes 55300
  161.7 26.1 %copy-start.15 = (f32[1,1,48,96]{3,2,1,0:T(8,128)S(1)}, f32[1,1,48,96]{3,2,1,0:T(8,128)}, u32[]{:S(2)}) copy-start(f32[1,1,48,96]{3,2,1,0:T(8,128)} %param.27) | copy-start | bytes 55300
  161.7 20.5 %all-to-all-start.5 = ((bf16[32,48,96]{2,1,0:T(8,128)(2,1)}), bf16[32,48,96]{2,1,0:T(8,128)(2,1)S(1)}, u32[]{:S(2)}, u32[]{:S(2)}) async-start(bf16[32,48,96]{2,1,0:T(8,128)(2,1)} %broadcast_in_dim.121), calls=%async_computation.5 | async-start | bytes 786432 | tf_op jit(solution)/shard_map/all_to_all | solution.py:168
  182.2 21.9 %all-to-all-start.4 = ((bf16[32,64,96]{2,1,0:T(8,128)(2,1)}), bf16[32,64,96]{2,1,0:T(8,128)(2,1)S(1)}, u32[]{:S(2)}, u32[]{:S(2)}) async-start(bf16[32,64,96]{2,1,0:T(8,128)(2,1)} %bitcast.33), calls=%async_computation.4 | async-start | bytes 1048576 | tf_op jit(solution)/shard_map/all_to_all | solution.py:170
where the time goes:
time: 206 us; the launch traced here: 205 us
  waiting for transfers between devices  55 us (27%)
  starting transfers between devices  50.6 us (25%)
  blocking collectives  47.7 us (23%)
  matrix products  22.4 us (11%)
  local copies, waits for them, and re-layouts  20 us (10%)
  other arithmetic  6.5 us (3%)
  between operations  2.54 us (1%)
    all_gather x1, blocking collectives, on_device(): grad_own = lax.all_gather(grad_part, 'y', axis=1, tiled=True)  28.7 us
    dot_general x30, matrix products, dot(): return lax.dot_general(a, b, dims, preferred_element_type=F32)  22.4 us
    all_gather x1, blocking collectives, on_device(): stream = lax.all_gather(stream_part, TP, axis=1, tiled=True)  19.1 us
    all_to_all x1, waiting for transfers between devices, on_device(): pieces = lax.all_to_all(pieces, 'y', 0, 0, tiled=True)  16.8 us
    all_to_all x1, waiting for transfers between devices, on_device(): lax.all_to_all(proj_part.reshape(sp_count, width // sp_count, value_dim),...  13.7 us
    all_to_all x1, starting transfers between devices, on_device(): got_grad = lax.all_to_all(send_grad, 'sp', 0, 0, tiled=True)  13.5 us
    all_to_all x1, waiting for transfers between devices, on_device(): states = lax.all_to_all(sent, 'sp', 0, 0, tiled=True)  12.9 us
    all_to_all x1, starting transfers between devices, on_device(): lax.all_to_all(share.reshape(sp_count, capacity, chunk), 'sp', 0, 0, tile...  9.71 us
  transfers between devices with their start and end apart: 9, of which 5 were waited for; matrix products, arithmetic and copies ran while one was open for 15% of the time, Pallas kernels for 0%

commit v1 on v0

--- a/solution.py
+++ b/solution.py
@@ -118,7 +118,9 @@
     rows_own = got_rows[:, :capacity].reshape(slot_count, -1)
     grad_part = got_grad[:, :capacity].reshape(slot_count, -1)
     ends = jnp.sum(got_grad[:, capacity, :3].astype(F32), axis=1)
-    grad_own = lax.all_gather(grad_part, "y", axis=1, tiled=True)
+    grad_own = jnp.concatenate(
+        lax.all_to_all(jnp.stack([grad_part] * lax.axis_size("y")), "y", 0, 0), axis=1
+    )
     rows_other = lax.ppermute(rows_own, "c", SWAP)
     grad_other = lax.ppermute(grad_own, "c", SWAP)
     gate_own, gate_other = (parity_rows(w_gate[0], k) for k in (core, 1 - core))

time: 206 us -> 229 us (1.11)
  waiting for transfers between devices: 55 us -> 92.8 us
  starting transfers between devices: 50.6 us -> 40.1 us
  blocking collectives: 47.7 us -> 41 us
    all_gather x1 -> x0, blocking collectives: 28.7 us -> none  [on_device(): grad_own = lax.all_gather(grad_part, 'y', axis=1, tiled=True)]
    all_to_all x0 -> x1, blocking collectives: none -> 22.3 us  [on_device(): got_grad = lax.all_to_all(send_grad, 'sp', 0, 0, tiled=True)]
    all_to_all x1, waiting for transfers between devices: 0.01 us -> 20.8 us  [on_device(): got_rows = lax.all_to_all(send_rows, 'sp', 0, 0, tiled=True)]
    all_to_all x1, waiting for transfers between devices: 4.32 us -> 21.4 us  [on_device(): lax.all_to_all(jnp.stack([grad_part] * lax.axis_size('y')), 'y', 0, 0)]
    all_to_all x1, starting transfers between devices: 13.5 us -> 7.1 us  [on_device(): lax.all_to_all(jnp.stack([grad_part] * lax.axis_size('y')), 'y', 0, 0)]
    all_to_all x1, starting transfers between devices: 9.71 us -> 5.57 us  [on_device(): lax.all_to_all(share.reshape(sp_count, capacity, chunk), 'sp', 0, 0, tile...]
  transfers between devices with their start and end apart: 9 -> 9, of which waited for: 5 -> 6; matrix products, arithmetic and copies ran while one was open for 15% -> 15% of each run, Pallas kernels for 0% -> 0%
where the time goes in v1:
time: 229 us; the launch traced here: 228 us
  waiting for transfers between devices  92.8 us (41%)
  blocking collectives  41 us (18%)
  starting transfers between devices  40.1 us (18%)
  matrix products  23.3 us (10%)
  local copies, waits for them, and re-layouts  22.2 us (10%)
  other arithmetic  5.85 us (3%)
  between operations  2.53 us (1%)
    dot_general x30, matrix products, dot(): return lax.dot_general(a, b, dims, preferred_element_type=F32)  23.3 us
    all_to_all x1, blocking collectives, on_device(): got_grad = lax.all_to_all(send_grad, 'sp', 0, 0, tiled=True)  22.3 us
    all_to_all x1, waiting for transfers between devices, on_device(): lax.all_to_all(jnp.stack([grad_part] * lax.axis_size('y')), 'y', 0, 0)  21.4 us
    all_to_all x1, waiting for transfers between devices, on_device(): got_rows = lax.all_to_all(send_rows, 'sp', 0, 0, tiled=True)  20.8 us
    all_gather x1, blocking collectives, on_device(): stream = lax.all_gather(stream_part, TP, axis=1, tiled=True)  18.7 us
    all_to_all x1, waiting for transfers between devices, on_device(): pieces = lax.all_to_all(pieces, 'y', 0, 0, tiled=True)  16.8 us
    all_to_all x1, waiting for transfers between devices, on_device(): lax.all_to_all(proj_part.reshape(sp_count, width // sp_count, value_dim),...  13.7 us
    all_to_all x1, waiting for transfers between devices, on_device(): states = lax.all_to_all(sent, 'sp', 0, 0, tiled=True)  12.9 us
  transfers between devices with their start and end apart: 9, of which 6 were waited for; matrix products, arithmetic and copies ran while one was open for 15% of the time, Pallas kernels for 0%

profile of v1, /device:TPU:2, one launch (start us, length us, event | category | flops | bytes accessed | tf_op | source)
XLA Modules:
  0.0 227.8 jit_solution(4255302092431208316)
XLA Ops:
  0.7 0.7 pad_bitcast_fusion
  2.0 0.6 slice.42
  3.9 0.8 fusion.41
  4.9 0.8 fusion.40
  5.6 0.8 multiply_add_fusion.1
  6.6 1.2 fusion.1
  7.9 22.3 %all_to_all.35 = bf16[32,16,128]{2,1,0:T(8,128)(2,1)S(1)} all-to-all(bf16[32,16,128]{2,1,0:T(8,128)(2,1)S(1)} %broadcast_select_fusion.4), channel_id=1, replica_groups=mesh['sp'=32,'y'=8,'c'=2] {'sp'}, dimensions={0} | all-to-all | bytes 262144 | tf_op jit(solution)/shard_map/all_to_all | solution.py:116
  30.2 1.1 stack.3
  31.3 7.1 %all-to-all-start.2 = ((bf16[8,480,128]{2,1,0:T(8,128)(2,1)}), bf16[8,480,128]{2,1,0:T(8,128)(2,1)S(1)}, u32[]{:S(2)}, u32[]{:S(2)}) async-start(bf16[8,480,128]{2,1,0:T(8,128)(2,1)} %stack.3), calls=%async_computation.2 | async-start | bytes 1966080 | tf_op jit(solution)/shard_map/all_to_all | solution.py:122
  38.4 0.6 reshape.292
  39.0 2.3 %dynamic-slice_reduce_fusion = bf16[192,8,128]{2,1,0:T(8,128)(2,1)S(1)} fusion(bf16[192,8,2,128]{3,2,1,0:T(2,128)(2,1)S(1)} %reshape.292, s32[]{:T(128)S(6)} %select_n.175), kind=kLoop, calls=%fused_computation.38 | loop fusion | bytes 786436 | tf_op jit(solution)/shard_map/jit(dynamic_index_in_dim)/dynamic_slice | solution.py:42
  41.4 1.6 convolution_convert_fusion.1
  42.9 21.4 %all-to-all-done.2 = bf16[8,480,128]{2,1,0:T(8,128)(2,1)S(1)} async-done(((bf16[8,480,128]{2,1,0:T(8,128)(2,1)}), bf16[8,480,128]{2,1,0:T(8,128)(2,1)S(1)}, u32[]{:S(2)}, u32[]{:S(2)}) %all-to-all-start.2) | async-done | bytes 983072 | tf_op jit(solution)/shard_map/all_to_all | solution.py:122
  64.3 5.4 %all-to-all-start = ((bf16[32,16,1024]{2,1,0:T(8,128)(2,1)}), bf16[32,16,1024]{2,1,0:T(8,128)(2,1)S(1)}, u32[]{:S(2)}, u32[]{:S(2)}) async-start(bf16[32,16,1024]{2,1,0:T(8,128)(2,1)} %bitcast.157), calls=%async_computation | async-start | bytes 2097152 | tf_op jit(solution)/shard_map/all_to_all | solution.py:117
  69.8 1.3 copy.49
  71.1 1.1 copy_bitcast_fusion
  72.2 1.9 collective-permute-start
  74.1 0.9 constant_dynamic-slice_fusion.4
  75.0 2.2 constant_dynamic-slice_fusion
  77.2 20.8 %all-to-all-done = bf16[32,16,1024]{2,1,0:T(8,128)(2,1)S(1)} async-done(((bf16[32,16,1024]{2,1,0:T(8,128)(2,1)}), bf16[32,16,1024]{2,1,0:T(8,128)(2,1)S(1)}, u32[]{:S(2)}, u32[]{:S(2)}) %all-to-all-start) | async-done | bytes 1048608 | tf_op jit(solution)/shard_map/all_to_all | solution.py:117
  98.3 2.1 collective-permute-start.1
  100.4 1.4 fusion.38
  101.8 1.4 fusion.45
  103.2 0.4 fusion.44
  103.6 1.7 convolution_add_fusion.2
  105.3 0.4 convolution_add_fusion
  105.8 1.1 multiply_convert_fusion
  106.9 0.4 fusion.47
  107.3 1.4 add_convert_fusion.1
  108.7 2.4 %collective-permute-start.2 = (bf16[480,1024]{1,0:T(8,128)(2,1)}, bf16[480,1024]{1,0:T(8,128)(2,1)}, u32[]{:S(2)}, u32[]{:S(2)}) collective-permute-start(bf16[480,1024]{1,0:T(8,128)(2,1)} %add_convert_fusion.1), channel_id=1, source_target_pairs={{0,1},{1,0},{2,3},{3,2},{4,5},{5,4},{6,7},{7,6},{8,9},{9,8},{10,11... | collective-permute-start | bytes 2949128 | tf_op jit(solution)/shard_map/ppermute | solution.py:140
  111.1 0.7 subtract_exponential_fusion
  111.8 1.2 fusion.27
  113.1 1.4 fusion.46
  114.5 1.6 fusion
  116.2 1.1 copy.71
  117.3 4.4 %all-to-all-start.3 = ((bf16[8,480,128]{2,1,0:T(8,128)(2,1)}), bf16[8,480,128]{2,1,0:T(8,128)(2,1)}, u32[]{:S(2)}, u32[]{:S(2)}) async-start(bf16[8,480,128]{2,1,0:T(8,128)(2,1)} %bitcast.149), calls=%async_computation.3 | async-start | bytes 1966080 | tf_op jit(solution)/shard_map/all_to_all | solution.py:144
  121.7 1.2 convolution_convert_fusion.3
  123.0 1.6 select_bitcast_fusion.1
  124.8 1.6 copy.52
  126.4 2.2 broadcast_in_dim_reshape.11
  128.6 0.5 convolution_convert_fusion.7
  129.1 0.5 convolution_convert_fusion.5
  129.6 0.5 broadcast_select_fusion.1
  130.1 0.5 broadcast_select_fusion.3
  130.6 16.8 %all-to-all-done.3 = bf16[8,480,128]{2,1,0:T(8,128)(2,1)} async-done(((bf16[8,480,128]{2,1,0:T(8,128)(2,1)}), bf16[8,480,128]{2,1,0:T(8,128)(2,1)}, u32[]{:S(2)}, u32[]{:S(2)}) %all-to-all-start.3) | async-done | bytes 983072 | tf_op jit(solution)/shard_map/all_to_all | solution.py:144
  147.4 1.3 reduce_sum.88
  148.7 0.7 reshape.308
  149.4 5.6 %all-to-all-start.4 = ((bf16[32,15,128]{2,1,0:T(8,128)(2,1)}), bf16[32,15,128]{2,1,0:T(8,128)(2,1)S(1)}, u32[]{:S(2)}, u32[]{:S(2)}) async-start(bf16[32,15,128]{2,1,0:T(8,128)(2,1)} %reshape.308), calls=%async_computation.4 | async-start | bytes 262144 | tf_op jit(solution)/shard_map/all_to_all | solution.py:159
  155.0 0.8 copy.50
  155.9 0.8 copy.51
  156.8 7.1 %all-to-all-done.4 = bf16[32,15,128]{2,1,0:T(8,128)(2,1)S(1)} async-done(((bf16[32,15,128]{2,1,0:T(8,128)(2,1)}), bf16[32,15,128]{2,1,0:T(8,128)(2,1)S(1)}, u32[]{:S(2)}, u32[]{:S(2)}) %all-to-all-start.4) | async-done | bytes 122912 | tf_op jit(solution)/shard_map/all_to_all | solution.py:159
  164.2 18.7 %all_gather.3 = bf16[192,2048]{1,0:T(8,128)(2,1)S(1)} all-gather(bf16[192,128]{1,0:T(8,128)(2,1)S(1)} %fusion.6), channel_id=1, replica_groups=mesh['sp'=32,'y'=8,'c'=2] {'y','c'}, dimensions={1}, use_global_device_ids=true | all-gather | bytes 835584 | tf_op jit(solution)/shard_map/all_gather | solution.py:163
  182.9 0.4 convolution_convert_fusion.8
  183.8 0.8 broadcast_in_dim.121
  184.6 5.6 %all-to-all-start.6 = ((bf16[32,48,96]{2,1,0:T(8,128)(2,1)}), bf16[32,48,96]{2,1,0:T(8,128)(2,1)S(1)}, u32[]{:S(2)}, u32[]{:S(2)}) async-start(bf16[32,48,96]{2,1,0:T(8,128)(2,1)} %broadcast_in_dim.121), calls=%async_computation.6 | async-start | bytes 786432 | tf_op jit(solution)/shard_map/all_to_all | solution.py:170
  190.6 1.0 copy.54
  191.7 0.5 fusion.2
  192.2 12.9 %all-to-all-done.6 = bf16[32,48,96]{2,1,0:T(8,128)(2,1)S(1)} async-done(((bf16[32,48,96]{2,1,0:T(8,128)(2,1)}), bf16[32,48,96]{2,1,0:T(8,128)(2,1)S(1)}, u32[]{:S(2)}, u32[]{:S(2)}) %all-to-all-start.6) | async-done | bytes 294944 | tf_op jit(solution)/shard_map/all_to_all | solution.py:170
  205.1 5.6 %all-to-all-start.5 = ((bf16[32,64,96]{2,1,0:T(8,128)(2,1)}), bf16[32,64,96]{2,1,0:T(8,128)(2,1)S(1)}, u32[]{:S(2)}, u32[]{:S(2)}) async-start(bf16[32,64,96]{2,1,0:T(8,128)(2,1)} %bitcast.34), calls=%async_computation.5 | async-start | bytes 1048576 | tf_op jit(solution)/shard_map/all_to_all | solution.py:172
  210.7 0.8 fusion.10
  211.7 0.8 fusion.11
  212.5 0.8 fusion.5
  213.3 13.7 %all-to-all-done.5 = bf16[32,64,96]{2,1,0:T(8,128)(2,1)S(1)} async-done(((bf16[32,64,96]{2,1,0:T(8,128)(2,1)}), bf16[32,64,96]{2,1,0:T(8,128)(2,1)S(1)}, u32[]{:S(2)}, u32[]{:S(2)}) %all-to-all-start.5) | async-done | bytes 393248 | tf_op jit(solution)/shard_map/all_to_all | solution.py:172
  227.0 0.7 convert_reduce_fusion
  (68 shorter events, 3.3 us)
Async XLA Ops:
  0.6 182.3 %copy-start = (bf16[96,2048]{1,0:T(8,128)(2,1)S(1)}, bf16[96,2048]{1,0:T(8,128)(2,1)}, u32[]{:S(2)}) copy-start(bf16[96,2048]{1,0:T(8,128)(2,1)} %param.21) | copy-start | bytes 1179652
  7.8 30.7 %copy-start.9 = (bf16[192,2048]{1,0:T(8,128)(2,1)S(1)}, bf16[192,2048]{1,0:T(8,128)(2,1)}, u32[]{:S(2)}) copy-start(bf16[192,2048]{1,0:T(8,128)(2,1)} %param.14) | copy-start | bytes 2359300
  30.1 8.3 %copy-start.10 = (bf16[32,16,128]{2,1,0:T(8,128)(2,1)}, bf16[32,16,128]{2,1,0:T(8,128)(2,1)S(1)}, u32[]{:S(2)}) copy-start(bf16[32,16,128]{2,1,0:T(8,128)(2,1)S(1)} %all_to_all.35) | copy-start | bytes 393220
  31.3 33.0 %all-to-all-start.2 = ((bf16[8,480,128]{2,1,0:T(8,128)(2,1)}), bf16[8,480,128]{2,1,0:T(8,128)(2,1)S(1)}, u32[]{:S(2)}, u32[]{:S(2)}) async-start(bf16[8,480,128]{2,1,0:T(8,128)(2,1)} %stack.3), calls=%async_computation.2 | async-start | bytes 1966080 | tf_op jit(solution)/shard_map/all_to_all | solution.py:122
  64.3 33.7 %all-to-all-start = ((bf16[32,16,1024]{2,1,0:T(8,128)(2,1)}), bf16[32,16,1024]{2,1,0:T(8,128)(2,1)S(1)}, u32[]{:S(2)}, u32[]{:S(2)}) async-start(bf16[32,16,1024]{2,1,0:T(8,128)(2,1)} %bitcast.157), calls=%async_computation | async-start | bytes 2097152 | tf_op jit(solution)/shard_map/all_to_all | solution.py:117
  72.2 31.4 %collective-permute-start = (bf16[480,1024]{1,0:T(8,128)(2,1)}, bf16[480,1024]{1,0:T(8,128)(2,1)}, u32[]{:S(2)}, u32[]{:S(2)}) collective-permute-start(bf16[480,1024]{1,0:T(8,128)(2,1)} %copy_bitcast_fusion), channel_id=1, source_target_pairs={{0,1},{1,0},{2,3},{3,2},{4,5},{5,4},{6,7},{7,6},{8,9},{9,8},{10,11... | collective-permute-start | bytes 2949128 | tf_op jit(solution)/shard_map/ppermute | solution.py:125
  98.3 4.9 %copy-start.1 = (bf16[8,1,128,128]{3,2,1,0:T(8,128)(2,1)S(1)}, bf16[8,1,128,128]{3,2,1,0:T(8,128)(2,1)}, u32[]{:S(2)}) copy-start(bf16[8,1,128,128]{3,2,1,0:T(8,128)(2,1)} %get-tuple-element.33) | copy-start | bytes 786436
  98.3 7.0 %collective-permute-start.1 = (bf16[480,1024]{1,0:T(8,128)(2,1)S(1)}, bf16[480,1024]{1,0:T(8,128)(2,1)S(1)}, u32[]{:S(2)}, u32[]{:S(2)}) collective-permute-start(bf16[480,1024]{1,0:T(8,128)(2,1)S(1)} %reshape.295), channel_id=1, source_target_pairs={{0,1},{1,0},{2,3},{3,2},{4,5},{5,4},{6,7},{7,6},{8,9},{9,8},{10,11... | collective-permute-start | bytes 2949128 | tf_op jit(solution)/shard_map/ppermute | solution.py:124
  100.4 3.3 %copy-start.7 = (bf16[128,8,1,128]{0,3,2,1:T(8,128)(2,1)S(1)}, bf16[128,8,1,128]{0,3,2,1:T(8,128)(2,1)}, u32[]{:S(2)}) copy-start(bf16[128,8,1,128]{0,3,2,1:T(8,128)(2,1)} %get-tuple-element.17) | copy-start | bytes 786436
  103.2 2.2 copy-start.3
  103.6 2.2 copy-start.8
  106.9 1.8 copy-start.4
  108.7 5.8 %collective-permute-start.2 = (bf16[480,1024]{1,0:T(8,128)(2,1)}, bf16[480,1024]{1,0:T(8,128)(2,1)}, u32[]{:S(2)}, u32[]{:S(2)}) collective-permute-start(bf16[480,1024]{1,0:T(8,128)(2,1)} %add_convert_fusion.1), channel_id=1, source_target_pairs={{0,1},{1,0},{2,3},{3,2},{4,5},{5,4},{6,7},{7,6},{8,9},{9,8},{10,11... | collective-permute-start | bytes 2949128 | tf_op jit(solution)/shard_map/ppermute | solution.py:140
  111.1 3.4 %copy-start.2 = (bf16[8,1,128,128]{3,2,1,0:T(8,128)(2,1)S(1)}, bf16[8,1,128,128]{3,2,1,0:T(8,128)(2,1)}, u32[]{:S(2)}) copy-start(bf16[8,1,128,128]{3,2,1,0:T(8,128)(2,1)} %get-tuple-element.33) | copy-start | bytes 786436
  111.1 3.4 %copy-start.5 = (bf16[480,128]{1,0:T(8,128)(2,1)S(1)}, bf16[480,128]{1,0:T(8,128)(2,1)}, u32[]{:S(2)}) copy-start(bf16[480,128]{1,0:T(8,128)(2,1)} %copy-done.4) | copy-start | bytes 368644
  117.3 30.1 %all-to-all-start.3 = ((bf16[8,480,128]{2,1,0:T(8,128)(2,1)}), bf16[8,480,128]{2,1,0:T(8,128)(2,1)}, u32[]{:S(2)}, u32[]{:S(2)}) async-start(bf16[8,480,128]{2,1,0:T(8,128)(2,1)} %bitcast.149), calls=%async_computation.3 | async-start | bytes 1966080 | tf_op jit(solution)/shard_map/all_to_all | solution.py:144
  124.7 4.3 %copy-start.6 = (bf16[480,128]{1,0:T(8,128)(2,1)S(1)}, bf16[480,128]{1,0:T(8,128)(2,1)}, u32[]{:S(2)}) copy-start(bf16[480,128]{1,0:T(8,128)(2,1)} %copy-done.4) | copy-start | bytes 368644
  149.4 14.5 %all-to-all-start.4 = ((bf16[32,15,128]{2,1,0:T(8,128)(2,1)}), bf16[32,15,128]{2,1,0:T(8,128)(2,1)S(1)}, u32[]{:S(2)}, u32[]{:S(2)}) async-start(bf16[32,15,128]{2,1,0:T(8,128)(2,1)} %reshape.308), calls=%async_computation.4 | async-start | bytes 262144 | tf_op jit(solution)/shard_map/all_to_all | solution.py:159
  155.0 8.9 %copy-start.16 = (bf16[192,128]{1,0:T(8,128)(2,1)S(1)}, bf16[192,128]{1,0:T(8,128)(2,1)}, u32[]{:S(2)}) copy-start(bf16[192,128]{1,0:T(8,128)(2,1)} %param.15) | copy-start | bytes 147460
  155.9 27.4 %copy-start.13 = (bf16[192,96]{1,0:T(8,128)(2,1)S(1)}, bf16[192,96]{1,0:T(8,128)(2,1)}, u32[]{:S(2)}) copy-start(bf16[192,96]{1,0:T(8,128)(2,1)} %param.22) | copy-start | bytes 110596
  163.9 19.7 %copy-start.11 = (bf16[192,48]{0,1:T(8,128)(2,1)S(1)}, bf16[192,48]{0,1:T(8,128)(2,1)}, u32[]{:S(2)}) copy-start(bf16[192,48]{0,1:T(8,128)(2,1)} %param.23) | copy-start | bytes 55300
  182.9 7.3 %copy-start.14 = (bf16[192,96]{1,0:T(8,128)(2,1)S(1)}, bf16[192,96]{1,0:T(8,128)(2,1)}, u32[]{:S(2)}) copy-start(bf16[192,96]{1,0:T(8,128)(2,1)} %param.25) | copy-start | bytes 110596
  183.3 8.3 %copy-start.12 = (bf16[192,48]{0,1:T(8,128)(2,1)S(1)}, bf16[192,48]{0,1:T(8,128)(2,1)}, u32[]{:S(2)}) copy-start(bf16[192,48]{0,1:T(8,128)(2,1)} %param.24) | copy-start | bytes 55300
  184.6 26.1 %copy-start.15 = (f32[1,1,48,96]{3,2,1,0:T(8,128)S(1)}, f32[1,1,48,96]{3,2,1,0:T(8,128)}, u32[]{:S(2)}) copy-start(f32[1,1,48,96]{3,2,1,0:T(8,128)} %param.27) | copy-start | bytes 55300
  184.6 20.5 %all-to-all-start.6 = ((bf16[32,48,96]{2,1,0:T(8,128)(2,1)}), bf16[32,48,96]{2,1,0:T(8,128)(2,1)S(1)}, u32[]{:S(2)}, u32[]{:S(2)}) async-start(bf16[32,48,96]{2,1,0:T(8,128)(2,1)} %broadcast_in_dim.121), calls=%async_computation.6 | async-start | bytes 786432 | tf_op jit(solution)/shard_map/all_to_all | solution.py:170
  205.1 21.9 %all-to-all-start.5 = ((bf16[32,64,96]{2,1,0:T(8,128)(2,1)}), bf16[32,64,96]{2,1,0:T(8,128)(2,1)S(1)}, u32[]{:S(2)}, u32[]{:S(2)}) async-start(bf16[32,64,96]{2,1,0:T(8,128)(2,1)} %bitcast.34), calls=%async_computation.5 | async-start | bytes 1048576 | tf_op jit(solution)/shard_map/all_to_all | solution.py:172
